TPU v7x, 32 devices: a whole 2x2x4 slice. The times are simulated.
32 devices in a mesh: fs: 8 (over z, y), tp: 4 (over x, core).
Axes of the slice: x: 2, y: 2, z: 4, core: 2. Of those that a mesh axis runs over, the one named last changes fastest.
Arguments:
- prompt_tokens: bfloat16 [768, 4096], P('tp'), may hold values from -6 to 6
- norm_gain: float32 [4096], P('fs'), may hold values from 0.1 to 1.9
- gate_trained: float32 [4096, 11264], P('fs', 'tp'), may hold values from -0.09375 to 0.09375
- up_trained: float32 [4096, 11264], P('fs', 'tp'), may hold values from -0.09375 to 0.09375
- down_trained: float32 [11264, 4096], P('fs', 'tp'), may hold values from -0.078125 to 0.078125
Outputs:
- gate_serving: bfloat16 [4096, 11264], P(None, 'fs')
- up_serving: bfloat16 [4096, 11264], P(None, 'fs')
- down_serving: bfloat16 [11264, 4096], P('fs')
- mixed: bfloat16 [768, 4096], P('tp', 'fs')
All inputs are finite; a program needn't handle non-finite values.
Results may differ from a plain program's by a relative error of at most 0.0082.
Values may be sent and summed in bfloat16 or wider, within the bound.
A program may use at most 128 MiB of HBM per device.

v0:
```python
import jax
import jax.numpy as jnp
from jax import lax
from jax.sharding import PartitionSpec as P


def on_device(prompt_tokens, norm_gain, gate_trained, up_trained, down_trained):
    fs_count = lax.axis_size("fs")
    gate_cast = (gate_trained * norm_gain[:, None]).astype(jnp.bfloat16)
    up_cast = (up_trained * norm_gain[:, None]).astype(jnp.bfloat16)
    down_cast = down_trained.astype(jnp.bfloat16)
    down_serving = lax.all_gather(down_cast, "tp", axis=1, tiled=True)
    gate_part, up_part = (
        lax.all_to_all(gate_cast, "tp", split_axis=0, concat_axis=1, tiled=True),
        lax.all_to_all(up_cast, "tp", split_axis=0, concat_axis=1, tiled=True),
    )
    gate_mid, up_mid = (
        lax.all_to_all(gate_part, "fs", split_axis=1, concat_axis=0, tiled=True),
        lax.all_to_all(up_part, "fs", split_axis=1, concat_axis=0, tiled=True),
    )
    share = gate_mid.shape[0] // fs_count
    width = gate_mid.shape[1]
    gate_blocks, up_blocks = (
        lax.all_gather(gate_mid.reshape(fs_count, share, width), "tp", axis=1, tiled=True),
        lax.all_gather(up_mid.reshape(fs_count, share, width), "tp", axis=1, tiled=True),
    )
    gate_serving = gate_blocks.reshape(-1, width)
    up_serving = up_blocks.reshape(-1, width)
    tokens = prompt_tokens.astype(jnp.float32)
    scale = lax.rsqrt(jnp.mean(tokens * tokens, axis=-1, keepdims=True) + 1e-06)
    normed = (tokens * scale).astype(jnp.bfloat16)
    contract = (((0,), (1,)), ((), ()))
    gate_cols = lax.dot_general(gate_serving, normed, contract, preferred_element_type=jnp.float32)
    up_cols = lax.dot_general(up_serving, normed, contract, preferred_element_type=jnp.float32)
    hidden_cols = (jax.nn.silu(gate_cols) * up_cols).astype(jnp.bfloat16)
    summed = lax.psum_scatter(
        lax.dot_general(
            down_serving, hidden_cols, (((0,), (0,)), ((), ())), preferred_element_type=jnp.float32
        ),
        "fs",
        scatter_dimension=0,
        tiled=True,
    )
    mixed = summed.T.astype(jnp.bfloat16)
    return (gate_serving, up_serving, down_serving, mixed)


def solution(mesh):
    return jax.shard_map(
        on_device,
        mesh=mesh,
        in_specs=(P("tp", None), P("fs"), P("fs", "tp"), P("fs", "tp"), P("fs", "tp")),
        out_specs=(P(None, "fs"), P(None, "fs"), P("fs", None), P("tp", "fs")),
        check_vma=False,
    )
```

profile of v0, /device:TPU:0, one launch (start us, length us, event | category | flops | bytes accessed | tf_op | source)
XLA Modules:
  0.0 524.6 jit_solution(6554279546055345411)
XLA Ops:
  7.2 0.0 all-gather.4.cloned.1.call-start
  7.2 5.5 %multiply_convert_fusion = (bf16[512,2816]{1,0:T(8,128)(2,1)S(1)}, bf16[512,2816]{1,0:T(8,128)(2,1)S(1)}) fusion(f32[512,2816]{1,0:T(8,128)} %param.8, f32[512]{0:T(512)} %param.6, f32[512,2816]{1,0:T(8,128)} %param.7), kind=kLoop, calls=%fused_computation | loop fusion | flops 5767168 | bytes 17303552 | tf_op jit(solution)/shard_map/convert_element_type | solution.py:10
  12.7 38.2 %all_to_all.64 = bf16[4,128,2816]{2,1,0:T(8,128)(2,1)} all-to-all(bf16[4,128,2816]{2,1,0:T(8,128)(2,1)S(1)} %bitcast.18), channel_id=1, replica_groups=mesh['fs'=8,'tp'=4] {'tp'}, dimensions={0} | all-to-all | bytes 5767168 | tf_op jit(solution)/shard_map/all_to_all | solution.py:14
  51.0 4.5 copy.9
  55.5 71.4 %all_to_all.65 = bf16[128,8,1408]{0,2,1:T(8,128)(2,1)} all-to-all(bf16[128,8,1408]{0,2,1:T(8,128)(2,1)} %bitcast.26), channel_id=1, replica_groups=mesh['fs'=8,'tp'=4] {'fs'}, dimensions={1} | all-to-all | bytes 5767168 | tf_op jit(solution)/shard_map/all_to_all | solution.py:18
  126.9 0.0 all-gather.4.cloned.1.call-update
  126.9 0.0 all-gather.6.cloned.1.call-start
  127.0 64.5 %all_to_all.66 = bf16[4,128,2816]{2,1,0:T(8,128)(2,1)} all-to-all(bf16[4,128,2816]{2,1,0:T(8,128)(2,1)S(1)} %bitcast.17), channel_id=1, replica_groups=mesh['fs'=8,'tp'=4] {'tp'}, dimensions={0} | all-to-all | bytes 5767168 | tf_op jit(solution)/shard_map/all_to_all | solution.py:15
  191.5 3.3 copy.11
  194.8 67.9 %all_to_all.67 = bf16[128,8,1408]{0,2,1:T(8,128)(2,1)} all-to-all(bf16[128,8,1408]{0,2,1:T(8,128)(2,1)S(1)} %bitcast.28), channel_id=1, replica_groups=mesh['fs'=8,'tp'=4] {'fs'}, dimensions={1} | all-to-all | bytes 5767168 | tf_op jit(solution)/shard_map/all_to_all | solution.py:19
  262.7 0.0 all-gather.6.cloned.1.call-update
  262.8 0.0 all-gather.8.cloned.1.call-start
  262.8 4.7 convert_element_type.26
  267.5 0.0 copy-start
  267.5 0.0 all-gather.8.cloned.1.call-update
  267.5 0.0 reduce-scatter.2.cloned.1.call-start
  267.6 1.6 copy-done
  269.1 0.4 fusion
  269.5 0.0 all-gather.4.cloned.1.call-done
  269.6 16.0 %copy.10 = bf16[8,512,1408]{2,1,0:T(8,128)(2,1)} copy(bf16[8,512,1408]{1,2,0:T(8,128)(2,1)} %all-gather.4.cloned.1.call-done) | data formatting | bytes 23068672 | tf_op jit(solution)/shard_map/all_gather | solution.py:24
  285.6 53.0 %all-gather.6.cloned.1.call-done = bf16[8,512,1408]{1,2,0:T(8,128)(2,1)} async-done(((bf16[8,128,1408]{1,2,0:T(8,128)(2,1)}), bf16[8,512,1408]{1,2,0:T(8,128)(2,1)}) %all-gather.6.cloned.1.call-update) | async-done | bytes 11534352 | tf_op jit(solution)/shard_map/all_gather | solution.py:25
  338.5 16.0 %copy.12 = bf16[8,512,1408]{2,1,0:T(8,128)(2,1)} copy(bf16[8,512,1408]{1,2,0:T(8,128)(2,1)} %all-gather.6.cloned.1.call-done) | data formatting | bytes 23068672 | tf_op jit(solution)/shard_map/all_gather | solution.py:25
  354.5 7.2 %fusion.3 = f32[1408,192]{0,1:T(8,128)S(1)} fusion(bf16[4096,1408]{1,0:T(8,128)(2,1)} %bitcast.19, bf16[192,4096]{1,0:T(8,128)(2,1)S(1)} %copy-done, f32[192]{0:T(256)S(1)} %add_rsqrt_fusion), kind=kOutput, calls=%fused_computation.9 | convolution fusion | flops 2216951808 | bytes 14189312 | tf_op jit(solution)/shard_map/dot_general | solution.py:33
  361.8 55.1 %all-gather.8.cloned.1.call-done = bf16[1408,4096]{1,0:T(8,128)(2,1)} async-done(((bf16[1408,1024]{1,0:T(8,128)(2,1)}), bf16[1408,4096]{1,0:T(8,128)(2,1)}) %all-gather.8.cloned.1.call-update) | async-done | bytes 11534352 | tf_op jit(solution)/shard_map/all_gather | solution.py:12
  416.8 14.4 %convolution_bitcast_fusion = f32[4096,192]{0,1:T(8,128)} fusion(bf16[1408,4096]{1,0:T(8,128)(2,1)} %all-gather.8.cloned.1.call-done, bf16[4096,1408]{1,0:T(8,128)(2,1)} %bitcast.21, f32[1408,192]{0,1:T(8,128)S(1)} %fusion.3, bf16[192,4096]{1,0:T(8,128)(2,1)S(1)} %copy-done, f32[192]{0:T(256)S(1)} %add_rsqrt_fusion), kind=kOutput, calls=%fused_computation.2 | convolution fusion | flops 4433166336 | bytes 28869376 | tf_op jit(solution)/shard_map/dot_general | solution.py:37
  431.3 0.0 reduce-scatter.2.cloned.1.call-update
  431.3 75.0 %reduce-scatter.2.cloned.1.call-done = f32[512,192]{0,1:T(8,128)} async-done(((f32[4096,192]{0,1:T(8,128)}), f32[512,192]{0,1:T(8,128)}) %reduce-scatter.2.cloned.1.call-update) | async-done | bytes 393232 | tf_op jit(solution)/shard_map/reduce_scatter | solution.py:36
  506.3 1.7 convert_bitcast_fusion
  508.0 10.1 %copy.14 = bf16[1408,4096]{1,0:T(8,128)(2,1)} copy(bf16[1408,4096]{1,0:T(8,128)(2,1)} %all-gather.8.cloned.1.call-done) | data formatting | bytes 23068672
  (1 shorter events, 0.0 us)
Async XLA Ops:
  7.2 262.4 %all-gather.4.cloned.1.call-start = ((), (), s32[]{:S(2)}) async-start(), calls=%async_computation.5 | async-start | bytes 14417920 | tf_op jit(solution)/shard_map/all_gather | solution.py:24
  126.9 211.6 %all-gather.6.cloned.1.call-start = ((), (), s32[]{:S(2)}) async-start(), calls=%async_computation.6 | async-start | bytes 14417920 | tf_op jit(solution)/shard_map/all_gather | solution.py:25
  262.8 154.1 %all-gather.8.cloned.1.call-start = ((), (), s32[]{:S(2)}) async-start(), calls=%async_computation.7 | async-start | bytes 14417920 | tf_op jit(solution)/shard_map/all_gather | solution.py:12
  267.5 1.6 copy-start
  267.5 238.8 %reduce-scatter.2.cloned.1.call-start = ((), (), s32[]{:S(2)}) async-start(), calls=%async_computation.8 | async-start | bytes 3538944 | tf_op jit(solution)/shard_map/reduce_scatter | solution.py:36
Sparse Core Ops, SparseCore 0:
  127.1 102.4 all-gather.3
  262.9 75.5 all-gather.5
  340.7 76.1 all-gather.7
  431.4 74.8 reduce-scatter.1
where the time goes:
time: 526 us; the launch traced here: 525 us
  blocking collectives  242 us (46%)
  waiting for transfers between devices  183 us (35%)
  local copies, waits for them, and re-layouts  51.5 us (10%)
  matrix products  21.7 us (4%)
  between operations  13.8 us (3%)
  other arithmetic  12.3 us (2%)
    reduce_scatter x1, waiting for transfers between devices, on_device(): lax.psum_scatter(lax.dot_general(down_serving, hidden_cols, (((0,), (0,))...  75 us
    all_to_all x1, blocking collectives, on_device(): lax.all_to_all(gate_part, 'fs', split_axis=1, concat_axis=0, tiled=True)  71.4 us
    all_to_all x1, blocking collectives, on_device(): lax.all_to_all(up_part, 'fs', split_axis=1, concat_axis=0, tiled=True)  67.9 us
    all_to_all x1, blocking collectives, on_device(): lax.all_to_all(up_cast, 'tp', split_axis=0, concat_axis=1, tiled=True)  64.5 us
    all_gather x1, waiting for transfers between devices, on_device(): down_serving = lax.all_gather(down_cast, 'tp', axis=1, tiled=True)  55.1 us
    all_gather x1, waiting for transfers between devices, on_device(): lax.all_gather(up_mid.reshape(fs_count, share, width), 'tp', axis=1, tile...  53 us
    all_to_all x1, blocking collectives, on_device(): lax.all_to_all(gate_cast, 'tp', split_axis=0, concat_axis=1, tiled=True)  38.2 us
    all_gather x1, local copies, waits for them, and re-layouts, on_device(): lax.all_gather(up_mid.reshape(fs_count, share, width), 'tp', axis=1, tile...  16 us
  transfers between devices with their start and end apart: 4, of which 3 were waited for; matrix products, arithmetic and copies ran while one was open for 9% of the time, Pallas kernels for 0%

commit v1 on v0

--- a/solution.py
+++ b/solution.py
@@ -2,6 +2,27 @@
 import jax.numpy as jnp
 from jax import lax
 from jax.sharding import PartitionSpec as P
+
+
+def _drive_block(mine, row_dim):
+    mine = jnp.moveaxis(mine, 0, row_dim)
+    tmp = mine.shape
+    everything = mine.reshape(*tmp[:row_dim], tmp[row_dim] * tmp[row_dim + 1], *tmp[row_dim + 2 :])
+    return everything
+
+
+def rest_local_data(local_values, axis_id):
+    aux = lax.axis_size(axis_id)
+    top, oldest = (aux, lax.axis_index(axis_id))
+    r_now, e_now = (local_values[None], 1)
+    while e_now < top:
+        front = map(lambda rr: (rr, rr ^ e_now), range(top))
+        back = lax.ppermute(r_now, axis_id, list(front))
+        long_array = oldest & e_now == 0
+        seen_now = jnp.where(long_array, r_now, back)
+        r_now = jnp.concatenate([seen_now, jnp.where(long_array, back, r_now)])
+        e_now *= 2
+    return r_now
 
 
 def on_device(prompt_tokens, norm_gain, gate_trained, up_trained, down_trained):
@@ -9,7 +30,8 @@
     gate_cast = (gate_trained * norm_gain[:, None]).astype(jnp.bfloat16)
     up_cast = (up_trained * norm_gain[:, None]).astype(jnp.bfloat16)
     down_cast = down_trained.astype(jnp.bfloat16)
-    down_serving = lax.all_gather(down_cast, "tp", axis=1, tiled=True)
+    heard = rest_local_data(down_cast, "tp")
+    down_serving = _drive_block(heard, 1)
     gate_part, up_part = (
         lax.all_to_all(gate_cast, "tp", split_axis=0, concat_axis=1, tiled=True),
         lax.all_to_all(up_cast, "tp", split_axis=0, concat_axis=1, tiled=True),

time: 526 us -> 606 us (1.15)
  waiting for transfers between devices: 183 us -> 256 us
  other arithmetic: 12.3 us -> 26 us
  local copies, waits for them, and re-layouts: 51.5 us -> 43.7 us
    ppermute x0 -> x2, waiting for transfers between devices: none -> 181 us  [rest_local_data(): back = lax.ppermute(r_now, axis_id, list(front))]
    all_gather x1 -> x0, waiting for transfers between devices: 55.1 us -> none  [on_device(): down_serving = lax.all_gather(down_cast, 'tp', axis=1, tiled=True)]
    all_gather x1, waiting for transfers between devices: 53 us -> 0.02 us  [on_device(): lax.all_gather(up_mid.reshape(fs_count, share, width), 'tp', axis=1, tile...]
    unnamed x3 -> x4, local copies, waits for them, and re-layouts: 11.7 us -> 0.15 us
    select_n x0 -> x2, other arithmetic: none -> 9.17 us  [rest_local_data(): seen_now = jnp.where(long_array, r_now, back)]
  transfers between devices with their start and end apart: 4 -> 5, of which waited for: 3 -> 3; matrix products, arithmetic and copies ran while one was open for 9% -> 8% of each run, Pallas kernels for 0% -> 0%
where the time goes in v1:
time: 606 us; the launch traced here: 605 us
  waiting for transfers between devices  256 us (42%)
  blocking collectives  242 us (40%)
  local copies, waits for them, and re-layouts  43.7 us (7%)
  other arithmetic  26 us (4%)
  matrix products  21.3 us (4%)
  between operations  13.8 us (2%)
    ppermute x2, waiting for transfers between devices, rest_local_data(): back = lax.ppermute(r_now, axis_id, list(front))  181 us
    reduce_scatter x1, waiting for transfers between devices, on_device(): lax.psum_scatter(lax.dot_general(down_serving, hidden_cols, (((0,), (0,))...  74.9 us
    all_to_all x1, blocking collectives, on_device(): lax.all_to_all(gate_part, 'fs', split_axis=1, concat_axis=0, tiled=True)  71.4 us
    all_to_all x1, blocking collectives, on_device(): lax.all_to_all(up_part, 'fs', split_axis=1, concat_axis=0, tiled=True)  67.9 us
    all_to_all x1, blocking collectives, on_device(): lax.all_to_all(up_cast, 'tp', split_axis=0, concat_axis=1, tiled=True)  64.5 us
    all_to_all x1, blocking collectives, on_device(): lax.all_to_all(gate_cast, 'tp', split_axis=0, concat_axis=1, tiled=True)  38.2 us
    all_gather x1, local copies, waits for them, and re-layouts, on_device(): lax.all_gather(gate_mid.reshape(fs_count, share, width), 'tp', axis=1, ti...  15.4 us
    all_gather x1, local copies, waits for them, and re-layouts, on_device(): lax.all_gather(up_mid.reshape(fs_count, share, width), 'tp', axis=1, tile...  15.3 us
  transfers between devices with their start and end apart: 5, of which 3 were waited for; matrix products, arithmetic and copies ran while one was open for 8% of the time, Pallas kernels for 0%

profile of v1, /device:TPU:0, one launch (start us, length us, event | category | flops | bytes accessed | tf_op | source)
XLA Modules:
  0.0 604.5 jit_solution(7218247534736713437)
XLA Ops:
  7.2 0.0 all-gather.3.cloned.1.call-start
  7.2 5.5 multiply_convert_fusion
  12.7 38.2 %all_to_all.64 = bf16[4,128,2816]{2,1,0:T(8,128)(2,1)} all-to-all(bf16[4,128,2816]{2,1,0:T(8,128)(2,1)S(1)} %bitcast.24), channel_id=1, replica_groups=mesh['fs'=8,'tp'=4] {'tp'}, dimensions={0} | all-to-all | bytes 5767168 | tf_op jit(solution)/shard_map/all_to_all | solution.py:36
  51.0 4.5 copy.11
  55.5 71.4 %all_to_all.65 = bf16[128,8,1408]{0,2,1:T(8,128)(2,1)} all-to-all(bf16[128,8,1408]{0,2,1:T(8,128)(2,1)} %bitcast.34), channel_id=1, replica_groups=mesh['fs'=8,'tp'=4] {'fs'}, dimensions={1} | all-to-all | bytes 5767168 | tf_op jit(solution)/shard_map/all_to_all | solution.py:40
  126.9 0.0 all-gather.3.cloned.1.call-update
  126.9 0.0 all-gather.5.cloned.1.call-start
  127.0 64.5 %all_to_all.66 = bf16[4,128,2816]{2,1,0:T(8,128)(2,1)} all-to-all(bf16[4,128,2816]{2,1,0:T(8,128)(2,1)S(1)} %bitcast.23), channel_id=1, replica_groups=mesh['fs'=8,'tp'=4] {'tp'}, dimensions={0} | all-to-all | bytes 5767168 | tf_op jit(solution)/shard_map/all_to_all | solution.py:37
  191.5 3.3 copy.13
  194.8 67.9 %all_to_all.67 = bf16[128,8,1408]{0,2,1:T(8,128)(2,1)} all-to-all(bf16[128,8,1408]{0,2,1:T(8,128)(2,1)S(1)} %bitcast.36), channel_id=1, replica_groups=mesh['fs'=8,'tp'=4] {'fs'}, dimensions={1} | all-to-all | bytes 5767168 | tf_op jit(solution)/shard_map/all_to_all | solution.py:41
  262.8 0.0 all-gather.5.cloned.1.call-update
  262.8 0.2 reduce-scatter.2.cloned.1.call-start
  263.0 3.1 convert_bitcast_fusion
  266.1 0.1 collective-permute-start
  266.2 5.5 collective-permute-done
  271.6 4.9 broadcast_select_fusion.3
  276.6 3.3 pad_maximum_fusion
  279.9 0.1 copy-done
  280.1 0.9 collective-permute-start.1
  281.0 1.8 fusion
  282.8 175.9 %collective-permute-done.1 = bf16[2,1408,1024]{2,1,0:T(8,128)(2,1)} collective-permute-done((bf16[2,1408,1024]{2,1,0:T(8,128)(2,1)}, bf16[2,1408,1024]{2,1,0:T(8,128)(2,1)}, u32[]{:S(2)}, u32[]{:S(2)}) %collective-permute-start.1) | collective-permute-done | bytes 5767200 | tf_op jit(solution)/shard_map/ppermute | solution.py:20
  458.8 4.2 broadcast_select_fusion.1
  463.0 1.4 maximum_bitcast_fusion
  464.4 5.0 copy.16
  469.4 15.4 %copy.12 = bf16[8,512,1408]{2,1,0:T(8,128)(2,1)} copy(bf16[8,512,1408]{1,2,0:T(8,128)(2,1)} %all-gather.3.cloned.1.call-done) | data formatting | bytes 23068672 | tf_op jit(solution)/shard_map/all_gather | solution.py:46
  484.8 6.9 %fusion.3 = f32[1408,192]{0,1:T(8,128)S(1)} fusion(bf16[4096,1408]{1,0:T(8,128)(2,1)} %bitcast.27, bf16[192,4096]{1,0:T(8,128)(2,1)S(1)} %copy-done.1, f32[192]{0:T(256)S(1)} %add_rsqrt_fusion), kind=kOutput, calls=%fused_computation.15 | convolution fusion | flops 2216951808 | bytes 14189312 | tf_op jit(solution)/shard_map/dot_general | solution.py:55
  491.7 0.0 all-gather.5.cloned.1.call-done
  491.7 15.3 %copy.14 = bf16[8,512,1408]{2,1,0:T(8,128)(2,1)} copy(bf16[8,512,1408]{1,2,0:T(8,128)(2,1)} %all-gather.5.cloned.1.call-done) | data formatting | bytes 23068672 | tf_op jit(solution)/shard_map/all_gather | solution.py:47
  507.0 14.3 %fusion.7 = f32[4096,192]{0,1:T(8,128)} fusion(bf16[1408,4096]{1,0:T(8,128)(2,1)} %bitcast.25, bf16[4096,1408]{1,0:T(8,128)(2,1)} %bitcast.29, f32[1408,192]{0,1:T(8,128)S(1)} %fusion.3, bf16[192,4096]{1,0:T(8,128)(2,1)S(1)} %copy-done.1, f32[192]{0:T(256)S(1)} %add_rsqrt_fusion), kind=kOutput, calls=%fused_computation.16 | convolution fusion | flops 4433166336 | bytes 28869376 | tf_op jit(solution)/shard_map/dot_general | solution.py:59
  521.3 0.0 reduce-scatter.2.cloned.1.call-update
  521.3 74.9 %reduce-scatter.2.cloned.1.call-done = f32[512,192]{0,1:T(8,128)} async-done(((f32[4096,192]{0,1:T(8,128)}), f32[512,192]{0,1:T(8,128)}) %reduce-scatter.2.cloned.1.call-update) | async-done | bytes 393232 | tf_op jit(solution)/shard_map/reduce_scatter | solution.py:58
  596.3 1.7 convert_bitcast_fusion.1
  (5 shorter events, 0.0 us)
Async XLA Ops:
  7.2 462.2 %all-gather.3.cloned.1.call-start = ((), (), s32[]{:S(2)}) async-start(), calls=%async_computation.5 | async-start | bytes 14417920 | tf_op jit(solution)/shard_map/all_gather | solution.py:46
  126.9 364.8 %all-gather.5.cloned.1.call-start = ((), (), s32[]{:S(2)}) async-start(), calls=%async_computation.6 | async-start | bytes 14417920 | tf_op jit(solution)/shard_map/all_gather | solution.py:47
  262.8 333.5 %reduce-scatter.2.cloned.1.call-start = ((), (), s32[]{:S(2)}) async-start(), calls=%async_computation.7 | async-start | bytes 3538944 | tf_op jit(solution)/shard_map/reduce_scatter | solution.py:58
  266.1 5.5 collective-permute-start
  276.6 3.5 copy-start
  280.1 178.7 %collective-permute-start.1 = (bf16[2,1408,1024]{2,1,0:T(8,128)(2,1)}, bf16[2,1408,1024]{2,1,0:T(8,128)(2,1)}, u32[]{:S(2)}, u32[]{:S(2)}) collective-permute-start(bf16[2,1408,1024]{2,1,0:T(8,128)(2,1)} %pad_maximum_fusion), channel_id=1, source_target_pairs={{0,2},{1,3},{2,0},{3,1},{4,6},{5,7},{6,4},{7,5},{8,10},{9,11},{10,... | collective-permute-start | bytes 17301512 | tf_op jit(solution)/shard_map/ppermute | solution.py:20
  469.4 15.4 %copy-start.1 = (bf16[192,4096]{1,0:T(8,128)(2,1)S(1)}, bf16[192,4096]{1,0:T(8,128)(2,1)}, u32[]{:S(2)}) copy-start(bf16[192,4096]{1,0:T(8,128)(2,1)} %param.5) | copy-start | bytes 4718596
Sparse Core Ops, SparseCore 0:
  127.1 102.4 all-gather.2
  262.9 127.5 all-gather.4
  521.5 74.7 reduce-scatter.1
